TPU v7x, 32 devices: a whole 2x2x4 slice. The times are simulated.
32 devices in a mesh: ep: 8 (over z, core), tp: 4 (over y, x).
Axes of the slice: x: 2, y: 2, z: 4, core: 2. Of those that a mesh axis runs over, the one named last changes fastest.
Arguments:
- tokens: bfloat16 [1536, 4096], P('ep'), may hold values from -6 to 6
- expert_ids: int32 [1536, 2], P('ep'), may hold values from 0 to 7, all different within a row; in each aligned block of 192 rows (0 to 191, 192 to 383, ...) at most 60 rows name the same one
- route_weight: float32 [1536, 2], P('ep'), may hold values from 0.1 to 1
- norm_gain: float32 [4096], replicated, may hold values from 0.1 to 1.9
- gate_weight: bfloat16 [8, 4096, 4096], P('ep', None, 'tp'), may hold values from -0.28125 to 0.28125
- up_weight: bfloat16 [8, 4096, 4096], P('ep', None, 'tp'), may hold values from -0.28125 to 0.28125
- down_weight: bfloat16 [8, 4096, 4096], P('ep', None, 'tp'), may hold values from -0.028076172 to 0.028076172
Outputs:
- mixed: bfloat16 [1536, 4096], P('ep', 'tp')
Inputs may be any that keep to these rules, and one draw needn't show every extreme that they name: `expert_ids`: each row names 2 different experts. In each aligned block of 192 rows (the tokens of one index of ep) no expert is named by more than 60 rows, and in some block some expert is named by exactly 60 rows.
All inputs are finite; a program needn't handle non-finite values.
Results may differ from a plain program's by a relative error of at most 0.007.
Values may be sent and summed in bfloat16 or wider, within the bound.
A program may use at most 64 MiB of HBM per device.

v0:
```python
import jax
import jax.numpy as jnp
from jax import lax
from jax.sharding import PartitionSpec as P

EPS = 1e-06
LIMIT = 7.0
ALPHA = 1.702


def rms_norm(tokens, norm_gain):
    values = tokens.astype(jnp.float32)
    scale = lax.rsqrt(jnp.mean(values * values, axis=-1, keepdims=True) + EPS)
    return (values * scale * norm_gain).astype(jnp.bfloat16)


def clamped_unit(gate_pre, up_pre):
    gate = jnp.minimum(gate_pre, LIMIT)
    up_part = jnp.clip(up_pre, -LIMIT, LIMIT)
    return ((up_part + 1.0) * gate * jax.nn.sigmoid(ALPHA * gate)).astype(jnp.bfloat16)


def slot_numbers(id_blocks, experts, capacity):
    onehot = (id_blocks[:, :, None] == jnp.arange(experts, dtype=jnp.int32)[None, None, :]).astype(
        jnp.int32
    )
    before = jnp.cumsum(onehot, axis=1) - onehot
    position = jnp.sum(before * onehot, axis=2)
    return id_blocks * capacity + position


def project_down(hidden, down_weight):
    result = jnp.einsum(
        "sejf,efd->sejd",
        lax.all_gather(hidden, "tp", axis=3, tiled=True),
        down_weight,
        preferred_element_type=jnp.float32,
    )
    return result.astype(jnp.bfloat16)


def on_device(tokens, expert_ids, route_weight, norm_gain, gate_weight, up_weight, down_weight):
    n_ep = lax.axis_size("ep")
    n_tp = lax.axis_size("tp")
    tok_rows, width = tokens.shape
    top = expert_ids.shape[1]
    local_experts = gate_weight.shape[0]
    experts = local_experts * n_ep
    capacity = 5 * tok_rows * top // (4 * experts)
    cols = width // n_tp
    normed = rms_norm(tokens, norm_gain)
    dest = slot_numbers(expert_ids.reshape(1, tok_rows * top), experts, capacity).reshape(-1)
    slot_range = jnp.arange(experts * capacity, dtype=jnp.int32)
    match = slot_range[:, None] == dest[None, :]
    pick = jnp.any(match.reshape(experts * capacity, tok_rows, top), axis=2).astype(jnp.bfloat16)
    own = lax.dynamic_slice_in_dim(normed, lax.axis_index("tp") * cols, cols, 1)
    buffer = jnp.dot(pick, own, preferred_element_type=jnp.float32).astype(jnp.bfloat16)
    buffer = buffer.reshape(n_ep, local_experts, capacity, cols)
    arrived = lax.all_to_all(buffer, "ep", split_axis=0, concat_axis=0, tiled=True)
    piece = lax.all_gather(arrived, "tp", axis=3, tiled=True)
    gate_part = jnp.einsum("sejd,edf->sejf", piece, gate_weight, preferred_element_type=jnp.float32)
    up_part = jnp.einsum("sejd,edf->sejf", piece, up_weight, preferred_element_type=jnp.float32)
    hidden = clamped_unit(gate_part, up_part)
    result = project_down(hidden, down_weight)
    back = lax.all_to_all(result, "ep", split_axis=0, concat_axis=0, tiled=True).reshape(
        experts * capacity, cols
    )
    chosen = jnp.transpose(match).astype(jnp.bfloat16)
    per_copy = jnp.dot(chosen, back, preferred_element_type=jnp.float32).reshape(
        tok_rows, top, cols
    )
    mixed = jnp.sum(per_copy * route_weight[:, :, None], axis=1)
    return mixed.astype(jnp.bfloat16)


def solution(mesh):
    placed = (
        P("ep", None),
        P("ep", None),
        P("ep", None),
        P(),
        P("ep", None, "tp"),
        P("ep", None, "tp"),
        P("ep", None, "tp"),
    )
    return jax.shard_map(
        on_device, mesh=mesh, in_specs=placed, out_specs=P("ep", "tp"), check_vma=False
    )
```

profile of v0, /device:TPU:0, one launch (start us, length us, event | category | flops | bytes accessed | tf_op | source)
XLA Modules:
  0.0 220.5 jit_solution(3522461065963199480)
XLA Ops:
  6.5 0.0 copy-start
  6.5 0.0 all-gather.3.cloned.1.call-start
  6.5 0.0 copy-start.1
  6.5 3.5 %convert_element_type.41 = f32[192,4096]{1,0:T(8,128)} convert(bf16[192,4096]{1,0:T(8,128)(2,1)} %param.7) | non-fusion elementwise | flops 786432 | bytes 4718592 | tf_op jit(solution)/shard_map/convert_element_type | solution.py:12
  10.1 0.0 copy-done
  10.1 0.4 multiply_reduce_fusion
  10.5 0.0 copy-done.1
  10.5 0.1 copy.28
  10.6 0.1 reshape.211
  10.8 0.9 reduce-window.6
  11.6 0.2 slice_reduce_fusion
  11.9 0.1 fusion.36
  12.0 0.1 reduce_sum.30
  12.1 0.1 copy.29
  12.2 0.2 fusion.30
  12.4 0.7 dynamic-slice
  13.1 1.6 convolution_convert_fusion
  14.8 0.2 reshape.217
  14.9 32.8 %all_to_all.10 = bf16[8,1,60,1024]{3,2,1,0:T(8,128)(2,1)} all-to-all(bf16[8,1,60,1024]{3,2,1,0:T(8,128)(2,1)S(1)} %bitcast.73), channel_id=1, replica_groups=mesh['ep'=8,'tp'=4] {'ep'}, dimensions={0} | all-to-all | bytes 1966080 | tf_op jit(solution)/shard_map/all_to_all | solution.py:59
  47.8 0.0 all-gather.3.cloned.1.call-update
  47.8 0.0 all-gather.5.cloned.1.call-start
  47.8 51.6 %all-gather.3.cloned.1.call-done = bf16[8,1,60,4096]{3,2,0,1:T(8,128)(2,1)} async-done(((bf16[8,1,60,1024]{3,2,0,1:T(8,128)(2,1)}), bf16[8,1,60,4096]{3,2,0,1:T(8,128)(2,1)}) %all-gather.3.cloned.1.call-update) | async-done | bytes 3932176 | tf_op jit(solution)/shard_map/all_gather | solution.py:60
  99.4 0.0 copy-start.2
  99.4 9.1 %fusion.2 = f32[8,60,1024]{2,1,0:T(8,128)S(1)} fusion(bf16[1,4096,1024]{2,1,0:T(8,128)(2,1)} %param.11, bf16[8,1,60,4096]{3,2,0,1:T(8,128)(2,1)} %all-gather.3.cloned.1.call-done), kind=kOutput, calls=%fused_computation.2 | convolution fusion | flops 4026531840 | bytes 14286848 | tf_op jit(solution)/shard_map/sejd,edf->sejf/dot_general | solution.py:61
  108.6 0.0 copy-done.2
  108.6 9.4 %fusion.23 = bf16[8,1,60,1024]{3,2,0,1:T(8,128)(2,1)} fusion(f32[8,60,1024]{2,1,0:T(8,128)S(1)} %fusion.2, bf16[1,4096,1024]{2,1,0:T(8,128)(2,1)} %param.12, bf16[8,1,60,4096]{3,2,0,1:T(8,128)(2,1)S(1)} %copy-done.2), kind=kOutput, calls=%fused_computation.15 | convolution fusion | flops 4031447040 | bytes 15269888 | tf_op jit(solution)/shard_map/sejd,edf->sejf/dot_general | solution.py:62
  118.0 0.0 all-gather.5.cloned.1.call-update
  118.0 52.7 %all-gather.5.cloned.1.call-done = bf16[8,1,60,4096]{3,2,0,1:T(8,128)(2,1)} async-done(((bf16[8,1,60,1024]{3,2,0,1:T(8,128)(2,1)}), bf16[8,1,60,4096]{3,2,0,1:T(8,128)(2,1)}) %all-gather.5.cloned.1.call-update) | async-done | bytes 3932176 | tf_op jit(solution)/shard_map/all_gather | solution.py:35
  170.7 10.1 %fusion.18 = bf16[8,1,60,1024]{3,2,1,0:T(8,128)(2,1)} fusion(bf16[1,4096,1024]{2,1,0:T(8,128)(2,1)} %param.13, bf16[8,1,60,4096]{3,2,0,1:T(8,128)(2,1)} %all-gather.5.cloned.1.call-done), kind=kOutput, calls=%fused_computation.14 | convolution fusion | flops 4027023360 | bytes 13303808 | tf_op jit(solution)/shard_map/sejf,efd->sejd/dot_general | solution.py:33
  180.8 0.0 copy-start.3
  180.8 4.7 %all-to-all-start.1 = ((bf16[8,1,60,1024]{3,2,1,0:T(8,128)(2,1)}), bf16[8,1,60,1024]{3,2,1,0:T(8,128)(2,1)S(1)}, u32[]{:S(2)}, u32[]{:S(2)}) async-start(bf16[8,1,60,1024]{3,2,1,0:T(8,128)(2,1)} %fusion.18), calls=%async_computation.1 | async-start | bytes 2097152 | tf_op jit(solution)/shard_map/all_to_all | solution.py:65
  185.6 0.2 iota_compare_fusion.1
  185.8 0.3 eq.60
  186.0 26.1 %all-to-all-done.1 = bf16[8,1,60,1024]{3,2,1,0:T(8,128)(2,1)S(1)} async-done(((bf16[8,1,60,1024]{3,2,1,0:T(8,128)(2,1)}), bf16[8,1,60,1024]{3,2,1,0:T(8,128)(2,1)S(1)}, u32[]{:S(2)}, u32[]{:S(2)}) %all-to-all-start.1) | async-done | bytes 983072 | tf_op jit(solution)/shard_map/all_to_all | solution.py:65
  212.1 0.2 reshape.235
  212.3 0.0 copy-done.3
  212.3 1.4 multiply_reduce_fusion.1
  (8 shorter events, 0.0 us)
Async XLA Ops:
  6.5 3.6 %copy-start = (bf16[192,4096]{1,0:T(8,128)(2,1)S(1)}, bf16[192,4096]{1,0:T(8,128)(2,1)}, u32[]{:S(2)}) copy-start(bf16[192,4096]{1,0:T(8,128)(2,1)} %param.7) | copy-start | bytes 4718596
  6.5 92.9 %all-gather.3.cloned.1.call-start = ((), (), s32[]{:S(2)}) async-start(), calls=%async_computation.2 | async-start | bytes 5242880 | tf_op jit(solution)/shard_map/all_gather | solution.py:60
  6.5 4.0 %copy-start.1 = (s32[192,2]{0,1:T(2,128)S(1)}, s32[192,2]{0,1:T(2,128)}, u32[]{:S(2)}) copy-start(s32[192,2]{0,1:T(2,128)} %param.8) | copy-start | bytes 4612
  47.8 122.9 %all-gather.5.cloned.1.call-start = ((), (), s32[]{:S(2)}) async-start(), calls=%async_computation.3 | async-start | bytes 5242880 | tf_op jit(solution)/shard_map/all_gather | solution.py:35
  99.4 9.1 %copy-start.2 = (bf16[8,1,60,4096]{3,2,0,1:T(8,128)(2,1)S(1)}, bf16[8,1,60,4096]{3,2,0,1:T(8,128)(2,1)}, u32[]{:S(2)}) copy-start(bf16[8,1,60,4096]{3,2,0,1:T(8,128)(2,1)} %all-gather.3.cloned.1.call-done) | copy-start | bytes 11796484
  180.8 31.5 %copy-start.3 = (f32[192,2]{0,1:T(2,128)S(1)}, f32[192,2]{0,1:T(2,128)}, u32[]{:S(2)}) copy-start(f32[192,2]{0,1:T(2,128)} %param.9) | copy-start | bytes 4612
  180.8 31.3 %all-to-all-start.1 = ((bf16[8,1,60,1024]{3,2,1,0:T(8,128)(2,1)}), bf16[8,1,60,1024]{3,2,1,0:T(8,128)(2,1)S(1)}, u32[]{:S(2)}, u32[]{:S(2)}) async-start(bf16[8,1,60,1024]{3,2,1,0:T(8,128)(2,1)} %fusion.18), calls=%async_computation.1 | async-start | bytes 2097152 | tf_op jit(solution)/shard_map/all_to_all | solution.py:65
Sparse Core Ops, SparseCore 0:
  47.9 51.4 all-gather.2
  118.1 52.5 all-gather.4
where the time goes:
time: 221 us
  waiting for transfers between devices  130 us (59%)
  blocking collectives  32.8 us (15%)
  matrix products  31.6 us (14%)
  between operations  13.5 us (6%)
  other arithmetic  5.26 us (2%)
  starting transfers between devices  4.78 us (2%)
    all_gather x1, waiting for transfers between devices, project_down(): lax.all_gather(hidden, 'tp', axis=3, tiled=True)  52.7 us
    all_gather x1, waiting for transfers between devices, on_device(): piece = lax.all_gather(arrived, 'tp', axis=3, tiled=True)  51.6 us
    all_to_all x1, blocking collectives, on_device(): lax.all_to_all(buffer, 'ep', split_axis=0, concat_axis=0, tiled=True)  32.8 us
    all_to_all x1, waiting for transfers between devices, on_device(): lax.all_to_all(result, 'ep', split_axis=0, concat_axis=0, tiled=True)  26.1 us
    dot_general x1, matrix products, project_down(): jnp.einsum('sejf,efd->sejd', lax.all_gather(hidden, 'tp', axis=3, tiled=T...  10.1 us
    dot_general x1, matrix products, on_device(): jnp.einsum('sejd,edf->sejf', piece, up_weight, preferred_element_type=jnp...  9.37 us
    dot_general x1, matrix products, on_device(): jnp.einsum('sejd,edf->sejf', piece, gate_weight, preferred_element_type=j...  9.13 us
    all_to_all x1, starting transfers between devices, on_device(): lax.all_to_all(result, 'ep', split_axis=0, concat_axis=0, tiled=True)  4.74 us
  transfers between devices with their start and end apart: 3, of which 3 were waited for; matrix products, arithmetic and copies ran while one was open for 0% of the time, Pallas kernels for 0%

commit v1 on v0

--- a/solution.py
+++ b/solution.py
@@ -1,6 +1,10 @@
+import functools
+
 import jax
 import jax.numpy as jnp
 from jax import lax
+from jax.experimental import pallas as pl
+from jax.experimental.pallas import tpu as pltpu
 from jax.sharding import PartitionSpec as P
 
 EPS = 1e-06
@@ -39,7 +43,7 @@
     return result.astype(jnp.bfloat16)
 
 
-def on_device(tokens, expert_ids, route_weight, norm_gain, gate_weight, up_weight, down_weight):
+def plain_path(tokens, expert_ids, route_weight, norm_gain, gate_weight, up_weight, down_weight):
     n_ep = lax.axis_size("ep")
     n_tp = lax.axis_size("tp")
     tok_rows, width = tokens.shape
@@ -73,6 +77,444 @@
     return mixed.astype(jnp.bfloat16)
 
 
+VMEM_BYTES = 60 * 1024 * 1024
+COLUMN_TILE = 256
+
+
+def flip(value, bits):
+    bit = 1
+    while bit <= bits:
+        if bits & bit:
+            value = value + bit - 2 * bit * lax.rem(lax.div(value, jnp.int32(bit)), jnp.int32(2))
+        bit *= 2
+    return value
+
+
+def fused_kernel(
+    n_ep,
+    n_tp,
+    slots,
+    tokens_ref,
+    ids_ref,
+    ids_row_ref,
+    route_ref,
+    gain_ref,
+    gate_hbm,
+    up_hbm,
+    down_hbm,
+    out_ref,
+    gate_v,
+    up_v,
+    down_v,
+    normed,
+    outbox,
+    fullbox,
+    xbuf,
+    hbuf,
+    obuf,
+    back,
+    weight_sem,
+    z_send,
+    z_recv,
+    pair_send,
+    pair_recv,
+    g_send,
+    g_recv,
+    b_send,
+    b_recv,
+):
+    pairs = n_ep // 2
+    tok_rows = tokens_ref.shape[0]
+    cols = xbuf.shape[-1]
+    hid = hbuf.shape[-1]
+    outs = obuf.shape[-1]
+    ep = lax.axis_index("ep")
+    tp = lax.axis_index("tp")
+    pair = lax.div(ep, jnp.int32(2))
+    core = lax.rem(ep, jnp.int32(2))
+    side = (flip(tp, 1), flip(tp, 2))
+    far = flip(tp, 3)
+
+    loads = [
+        pltpu.make_async_copy(hbm.at[0], vmem, weight_sem.at[i])
+        for i, (hbm, vmem) in enumerate(((gate_hbm, gate_v), (up_hbm, up_v), (down_hbm, down_v)))
+    ]
+    for load in loads:
+        load.start()
+
+    barrier = pltpu.get_barrier_semaphore()
+    for k in range(1, n_ep):
+        pl.semaphore_signal(
+            barrier, inc=1, device_id=(flip(ep, k), tp), device_id_type=pl.DeviceIdType.MESH
+        )
+    for other in side:
+        pl.semaphore_signal(
+            barrier, inc=1, device_id=(ep, other), device_id_type=pl.DeviceIdType.MESH
+        )
+
+    def norm_rows(i, carry):
+        rows = pl.ds(pl.multiple_of(i * 16, 16), 16)
+        values = tokens_ref[rows, :].astype(jnp.float32)
+        scale = lax.rsqrt(jnp.mean(values * values, axis=-1, keepdims=True) + EPS)
+        normed[rows, :] = (values * scale * gain_ref[...]).astype(jnp.bfloat16)
+        return carry
+
+    lax.fori_loop(0, tok_rows // 16, norm_rows, 0)
+
+    ids_row = ids_row_ref[...]
+    expert_col = lax.broadcasted_iota(jnp.int32, (n_ep, tok_rows), 0)
+    hits_row = ((ids_row[0:1, :] == expert_col) | (ids_row[1:2, :] == expert_col)).astype(
+        jnp.float32
+    ).astype(jnp.bfloat16)
+    first = lax.broadcasted_iota(jnp.int32, (tok_rows, tok_rows), 0)
+    second = lax.broadcasted_iota(jnp.int32, (tok_rows, tok_rows), 1)
+    earlier = (first < second).astype(jnp.float32).astype(jnp.bfloat16)
+    before_row = jnp.dot(hits_row, earlier, preferred_element_type=jnp.float32)
+    slot_row = [
+        jnp.sum(jnp.where(ids_row[k : k + 1, :] == expert_col, before_row, 0.0), axis=0, keepdims=True)
+        for k in range(2)
+    ]
+    slot_at = lax.broadcasted_iota(jnp.int32, (slots, tok_rows), 0).astype(jnp.float32)
+
+    def pick_of(expert):
+        taken = ((ids_row[0:1, :] == expert) & (slot_row[0] == slot_at)) | (
+            (ids_row[1:2, :] == expert) & (slot_row[1] == slot_at)
+        )
+        return taken.astype(jnp.float32).astype(jnp.bfloat16)
+
+    pl.semaphore_wait(barrier, n_ep - 1 + 2)
+
+    own_cols = pl.ds(pl.multiple_of(tp * cols, cols), cols)
+
+    def z_copy(k, c):
+        return pltpu.make_async_remote_copy(
+            src_ref=outbox.at[k - 1, c],
+            dst_ref=xbuf.at[k, tp, core],
+            send_sem=z_send.at[k, c],
+            recv_sem=z_recv.at[k, core],
+            device_id=(flip(pair, k) * 2 + c, tp),
+            device_id_type=pl.DeviceIdType.MESH,
+        )
+
+    def z_arrival(k, c):
+        return pltpu.make_async_remote_copy(
+            src_ref=outbox.at[k - 1, c],
+            dst_ref=xbuf.at[k, tp, c],
+            send_sem=z_send.at[k, c],
+            recv_sem=z_recv.at[k, c],
+            device_id=(flip(pair, k) * 2 + c, tp),
+            device_id_type=pl.DeviceIdType.MESH,
+        )
+
+    for k in range(1, pairs):
+        for c in range(2):
+            outbox[k - 1, c] = jnp.dot(
+                pick_of(flip(pair, k) * 2 + c),
+                normed[:, own_cols],
+                preferred_element_type=jnp.float32,
+            ).astype(jnp.bfloat16)
+            z_copy(k, c).start()
+
+    partner = flip(ep, 1)
+    pair_copy = pltpu.make_async_remote_copy(
+        src_ref=fullbox,
+        dst_ref=xbuf.at[0, :, core],
+        send_sem=pair_send,
+        recv_sem=pair_recv,
+        device_id=(partner, tp),
+        device_id_type=pl.DeviceIdType.MESH,
+    )
+    pair_arrival = pltpu.make_async_remote_copy(
+        src_ref=fullbox,
+        dst_ref=xbuf.at[0, :, 1 - core],
+        send_sem=pair_send,
+        recv_sem=pair_recv,
+        device_id=(partner, tp),
+        device_id_type=pl.DeviceIdType.MESH,
+    )
+    theirs = pick_of(partner)
+    for j in range(n_tp):
+        fullbox[j] = jnp.dot(
+            theirs, normed[:, j * cols : (j + 1) * cols], preferred_element_type=jnp.float32
+        ).astype(jnp.bfloat16)
+    pair_copy.start()
+    mine = pick_of(ep)
+    for j in range(n_tp):
+        xbuf[0, j, core] = jnp.dot(
+            mine, normed[:, j * cols : (j + 1) * cols], preferred_element_type=jnp.float32
+        ).astype(jnp.bfloat16)
+
+    boxes = (xbuf, hbuf)
+
+    def block_copy(b, k, d, half):
+        return pltpu.make_async_remote_copy(
+            src_ref=boxes[b].at[k, tp, half],
+            dst_ref=boxes[b].at[k, tp, half],
+            send_sem=g_send.at[b, k, 2 * d + half],
+            recv_sem=g_recv.at[b, k, 2 * d + half],
+            device_id=(ep, side[d]),
+            device_id_type=pl.DeviceIdType.MESH,
+        )
+
+    def block_arrival(b, k, d, half):
+        return pltpu.make_async_remote_copy(
+            src_ref=boxes[b].at[k, side[d], half],
+            dst_ref=boxes[b].at[k, side[d], half],
+            send_sem=g_send.at[b, k, 2 * d + half],
+            recv_sem=g_recv.at[b, k, 2 * d + half],
+            device_id=(ep, side[d]),
+            device_id_type=pl.DeviceIdType.MESH,
+        )
+
+    def relay_copy(b, k, d):
+        return pltpu.make_async_remote_copy(
+            src_ref=boxes[b].at[k, side[d], d],
+            dst_ref=boxes[b].at[k, side[d], d],
+            send_sem=g_send.at[b, k, 4 + d],
+            recv_sem=g_recv.at[b, k, 4 + d],
+            device_id=(ep, side[1 - d]),
+            device_id_type=pl.DeviceIdType.MESH,
+        )
+
+    def relay_arrival(b, k, d):
+        return pltpu.make_async_remote_copy(
+            src_ref=boxes[b].at[k, far, d],
+            dst_ref=boxes[b].at[k, far, d],
+            send_sem=g_send.at[b, k, 4 + d],
+            recv_sem=g_recv.at[b, k, 4 + d],
+            device_id=(ep, side[1 - d]),
+            device_id_type=pl.DeviceIdType.MESH,
+        )
+
+    def spread(b, k):
+        for step in range(2):
+            for d in range(2):
+                block_copy(b, k, d, d if step == 0 else 1 - d).start()
+
+    def relay(b, k):
+        for d in range(2):
+            block_arrival(b, k, d, d).wait_recv()
+            relay_copy(b, k, d).start()
+
+    def gathered(b, k):
+        for d in range(2):
+            block_arrival(b, k, d, 1 - d).wait_recv()
+        for d in range(2):
+            relay_arrival(b, k, d).wait_recv()
+
+    def enter(k):
+        for c in range(2):
+            z_arrival(k, c).wait_recv()
+        spread(0, k)
+
+    def dot_blocks(box, k, weight, where):
+        depth = box.shape[-1]
+        total = None
+        for j in range(n_tp):
+            part = jnp.dot(
+                box[k, j].reshape(2 * slots, depth),
+                weight[j * depth : (j + 1) * depth, where],
+                preferred_element_type=jnp.float32,
+            )
+            total = part if total is None else total + part
+        return total
+
+    def units(k):
+        def tile(i, carry):
+            where = pl.ds(pl.multiple_of(i * COLUMN_TILE, COLUMN_TILE), COLUMN_TILE)
+            gate_pre = dot_blocks(xbuf, k, gate_v, where)
+            up_pre = dot_blocks(xbuf, k, up_v, where)
+            hidden = clamped_unit(gate_pre, up_pre)
+            hbuf[k, tp, :, :, where] = hidden.reshape(2, slots, COLUMN_TILE)
+            return carry
+
+        lax.fori_loop(0, hid // COLUMN_TILE, tile, 0)
+        spread(1, k)
+
+    def back_copy(k, c):
+        return pltpu.make_async_remote_copy(
+            src_ref=obuf.at[k, c],
+            dst_ref=back.at[ep],
+            send_sem=b_send.at[k, c],
+            recv_sem=b_recv.at[ep],
+            device_id=(flip(pair, k) * 2 + c, tp),
+            device_id_type=pl.DeviceIdType.MESH,
+        )
+
+    def back_arrival(flips):
+        other = flip(ep, flips)
+        return pltpu.make_async_remote_copy(
+            src_ref=obuf.at[0, 0],
+            dst_ref=back.at[other],
+            send_sem=b_send.at[0, 0],
+            recv_sem=b_recv.at[other],
+            device_id=(other, tp),
+            device_id_type=pl.DeviceIdType.MESH,
+        )
+
+    partner_back = pltpu.make_async_remote_copy(
+        src_ref=obuf.at[0, 1 - core],
+        dst_ref=back.at[ep],
+        send_sem=b_send.at[0, 0],
+        recv_sem=b_recv.at[ep],
+        device_id=(partner, tp),
+        device_id_type=pl.DeviceIdType.MESH,
+    )
+
+    def results(k):
+        def tile(i, carry):
+            where = pl.ds(pl.multiple_of(i * COLUMN_TILE, COLUMN_TILE), COLUMN_TILE)
+            total = dot_blocks(hbuf, k, down_v, where).astype(jnp.bfloat16)
+            obuf[k, :, :, where] = total.reshape(2, slots, COLUMN_TILE)
+            return carry
+
+        lax.fori_loop(0, outs // COLUMN_TILE, tile, 0)
+        if k == 0:
+            partner_back.start()
+            back[ep] = obuf[0, core]
+        else:
+            for c in range(2):
+                back_copy(k, c).start()
+
+    loads[0].wait()
+    loads[1].wait()
+    pair_arrival.wait_recv()
+    units(0)
+    enter(1)
+    relay(1, 0)
+    if pairs > 2:
+        enter(2)
+    relay(0, 1)
+    loads[2].wait()
+    gathered(1, 0)
+    results(0)
+    for k in range(1, pairs):
+        gathered(0, k)
+        units(k)
+        if k + 2 < pairs:
+            enter(k + 2)
+        if k + 1 < pairs:
+            relay(0, k + 1)
+            relay(1, k)
+        if k >= 2:
+            gathered(1, k - 1)
+            results(k - 1)
+    relay(1, pairs - 1)
+    gathered(1, pairs - 1)
+    results(pairs - 1)
+
+    expert_row = lax.broadcasted_iota(jnp.int32, (tok_rows, n_ep), 1)
+    ids = [ids_ref[:, k : k + 1] for k in range(2)]
+    hits = ((ids[0] == expert_row) | (ids[1] == expert_row)).astype(jnp.float32).astype(jnp.bfloat16)
+    later = (second < first).astype(jnp.float32).astype(jnp.bfloat16)
+    before = jnp.dot(later, hits, preferred_element_type=jnp.float32)
+    place = lax.broadcasted_iota(jnp.int32, (tok_rows, n_ep * slots), 1).astype(jnp.float32)
+    chosen = []
+    for k in range(2):
+        slot = jnp.sum(jnp.where(ids[k] == expert_row, before, 0.0), axis=1, keepdims=True)
+        spot = ids[k].astype(jnp.float32) * slots + slot
+        chosen.append((place == spot).astype(jnp.float32).astype(jnp.bfloat16))
+
+    for flips in range(1, n_ep):
+        back_arrival(flips).wait_recv()
+
+    def mix(i, carry):
+        where = pl.ds(pl.multiple_of(i * COLUMN_TILE, COLUMN_TILE), COLUMN_TILE)
+        table = back[:, :, where].reshape(n_ep * slots, COLUMN_TILE)
+        total = None
+        for k in range(2):
+            part = jnp.dot(chosen[k], table, preferred_element_type=jnp.float32)
+            part = part * route_ref[:, k : k + 1]
+            total = part if total is None else total + part
+        out_ref[:, where] = total.astype(jnp.bfloat16)
+        return carry
+
+    lax.fori_loop(0, outs // COLUMN_TILE, mix, 0)
+
+    for k in range(1, pairs):
+        for c in range(2):
+            z_copy(k, c).wait_send()
+            back_copy(k, c).wait_send()
+    pair_copy.wait_send()
+    partner_back.wait_send()
+    for k in range(pairs):
+        for b in range(2):
+            if b == 0 and k == 0:
+                continue
+            for d in range(2):
+                for half in range(2):
+                    block_copy(b, k, d, half).wait_send()
+                relay_copy(b, k, d).wait_send()
+
+
+def fused_path(
+    n_ep, n_tp, tokens, expert_ids, route_weight, norm_gain, gate_weight, up_weight, down_weight
+):
+    tok_rows, width = tokens.shape
+    slots = slots_of(n_ep, tokens.shape, expert_ids.shape)
+    hid = gate_weight.shape[2]
+    outs = down_weight.shape[2]
+    cols = width // n_tp
+    pairs = n_ep // 2
+    vmem = pl.BlockSpec(memory_space=pltpu.VMEM)
+    hbm = pl.BlockSpec(memory_space=pl.ANY)
+    dma = pltpu.SemaphoreType.DMA
+    return pl.pallas_call(
+        functools.partial(fused_kernel, n_ep, n_tp, slots),
+        out_shape=jax.ShapeDtypeStruct((tok_rows, outs), jnp.bfloat16),
+        in_specs=[vmem] * 5 + [hbm] * 3,
+        out_specs=vmem,
+        scratch_shapes=[
+            pltpu.VMEM(gate_weight.shape[1:], jnp.bfloat16),
+            pltpu.VMEM(up_weight.shape[1:], jnp.bfloat16),
+            pltpu.VMEM(down_weight.shape[1:], jnp.bfloat16),
+            pltpu.VMEM((tok_rows, width), jnp.bfloat16),
+            pltpu.VMEM((pairs - 1, 2, slots, cols), jnp.bfloat16),
+            pltpu.VMEM((n_tp, slots, cols), jnp.bfloat16),
+            pltpu.VMEM((pairs, n_tp, 2, slots, cols), jnp.bfloat16),
+            pltpu.VMEM((pairs, n_tp, 2, slots, hid), jnp.bfloat16),
+            pltpu.VMEM((pairs, 2, slots, outs), jnp.bfloat16),
+            pltpu.VMEM((n_ep, slots, outs), jnp.bfloat16),
+            dma((3,)),
+            dma((pairs, 2)),
+            dma((pairs, 2)),
+            dma,
+            dma,
+            dma((2, pairs, 6)),
+            dma((2, pairs, 6)),
+            dma((pairs, 2)),
+            dma((n_ep,)),
+        ],
+        compiler_params=pltpu.CompilerParams(
+            collective_id=0, has_side_effects=True, vmem_limit_bytes=VMEM_BYTES
+        ),
+    )(
+        tokens,
+        expert_ids,
+        jnp.transpose(expert_ids),
+        route_weight,
+        norm_gain.reshape(1, width),
+        gate_weight,
+        up_weight,
+        down_weight,
+    )
+
+
+def slots_of(n_ep, token_shape, id_shape):
+    capacity = 5 * token_shape[0] * id_shape[1] // (4 * n_ep)
+    return -(-capacity // 16) * 16
+
+
+def on_device(tokens, expert_ids, route_weight, norm_gain, gate_weight, up_weight, down_weight):
+    n_ep = lax.axis_size("ep")
+    n_tp = lax.axis_size("tp")
+    args = (tokens, expert_ids, route_weight, norm_gain, gate_weight, up_weight, down_weight)
+    fits = n_tp == 4 and n_ep >= 4 and n_ep & (n_ep - 1) == 0 and gate_weight.shape[0] == 1
+    if fits and expert_ids.shape[1] == 2:
+        return fused_path(n_ep, n_tp, *args)
+    return plain_path(*args)
+
+
 def solution(mesh):
     placed = (
         P("ep", None),

time: 221 us -> 102 us (0.46)
  the two profiles are of different devices: /device:TPU:0 before, /device:TPU:19 now
where the time goes in v1:
time: 102 us
  Pallas kernels  97.4 us (95%)
  local copies, waits for them, and re-layouts  4.65 us (5%)
    pallas_call x1, Pallas kernels, fused_path(): pl.pallas_call(functools.partial(fused_kernel, n_ep, n_tp, slots), out_sh...  97.4 us
    unnamed x3, local copies, waits for them, and re-layouts  4.65 us

profile of v1, /device:TPU:19, one launch (start us, length us, event | category | flops | bytes accessed | tf_op | source)
XLA Modules:
  0.0 102.0 jit_solution(17467023456232359770)
XLA Ops:
  0.0 1.4 %copy.9.route_ref = f32[192,2]{1,0:T(8,128)} copy(f32[192,2]{0,1:T(2,128)} %param.9) | data formatting | bytes 3072 | tf_op args[2]
  1.4 1.4 %copy.8.ids_ref = s32[192,2]{1,0:T(8,128)} copy(s32[192,2]{0,1:T(2,128)} %param.8) | data formatting | bytes 3072 | tf_op args[1]
  2.9 97.4 %shard_map.73 = bf16[192,1024]{1,0:T(8,128)(2,1)} custom-call(bf16[192,4096]{1,0:T(8,128)(2,1)} %tokens_ref.1, s32[192,2]{1,0:T(8,128)} %copy.8.ids_ref, s32[2,192]{1,0:T(2,128)} %bitcast.3, f32[192,2]{1,0:T(8,128)} %copy.9.route_ref, f32[1,4096]{1,0:T(1,128)} %bitcast.2, bf16[1,4096,1024]{2,1,0:T(8,128)(2,1)} %gate_hbm.1, bf16[1,4096,1024]{2,1,0:T(8,128)(2,1)} %up_hbm.1, ...), custom_call_target="tpu_custom_call" | custom-call | tf_op jit(solution)/shard_map/pallas_call | solution.py:462
  100.3 1.8 %copy.11 = bf16[192,1024]{1,0:T(8,128)(2,1)} copy(bf16[192,1024]{1,0:T(8,128)(2,1)} %shard_map.73) | data formatting | bytes 786432

commit v2 on v1

--- a/solution.py
+++ b/solution.py
@@ -77,7 +77,7 @@
     return mixed.astype(jnp.bfloat16)
 
 
-VMEM_BYTES = 60 * 1024 * 1024
+VMEM_BYTES = 46 * 1024 * 1024
 COLUMN_TILE = 256
 
 
@@ -94,18 +94,22 @@
     n_ep,
     n_tp,
     slots,
-    tokens_ref,
-    ids_ref,
-    ids_row_ref,
-    route_ref,
-    gain_ref,
+    tokens_hbm,
+    ids_row_hbm,
+    route_row_hbm,
+    gain_hbm,
     gate_hbm,
     up_hbm,
     down_hbm,
     out_ref,
+    tokens_ref,
+    ids_row_ref,
+    route_row_ref,
+    gain_ref,
     gate_v,
     up_v,
     down_v,
+    scales,
     normed,
     outbox,
     fullbox,
@@ -113,6 +117,7 @@
     hbuf,
     obuf,
     back,
+    small_sem,
     weight_sem,
     z_send,
     z_recv,
@@ -135,6 +140,17 @@
     side = (flip(tp, 1), flip(tp, 2))
     far = flip(tp, 3)
 
+    small = (
+        (tokens_hbm, tokens_ref),
+        (ids_row_hbm, ids_row_ref),
+        (route_row_hbm, route_row_ref),
+        (gain_hbm, gain_ref),
+    )
+    small_loads = [
+        pltpu.make_async_copy(a, b, small_sem.at[i]) for i, (a, b) in enumerate(small)
+    ]
+    for load in small_loads:
+        load.start()
     loads = [
         pltpu.make_async_copy(hbm.at[0], vmem, weight_sem.at[i])
         for i, (hbm, vmem) in enumerate(((gate_hbm, gate_v), (up_hbm, up_v), (down_hbm, down_v)))
@@ -152,14 +168,21 @@
             barrier, inc=1, device_id=(ep, other), device_id_type=pl.DeviceIdType.MESH
         )
 
-    def norm_rows(i, carry):
+    for load in small_loads:
+        load.wait()
+
+    own_cols = pl.ds(pl.multiple_of(tp * cols, cols), cols)
+
+    def scale_rows(i, carry):
         rows = pl.ds(pl.multiple_of(i * 16, 16), 16)
         values = tokens_ref[rows, :].astype(jnp.float32)
         scale = lax.rsqrt(jnp.mean(values * values, axis=-1, keepdims=True) + EPS)
-        normed[rows, :] = (values * scale * gain_ref[...]).astype(jnp.bfloat16)
+        scales[rows, :] = jnp.broadcast_to(scale, (16, scales.shape[1]))
+        values = tokens_ref[rows, own_cols].astype(jnp.float32)
+        normed[rows, own_cols] = (values * scale * gain_ref[:, own_cols]).astype(jnp.bfloat16)
         return carry
 
-    lax.fori_loop(0, tok_rows // 16, norm_rows, 0)
+    lax.fori_loop(0, tok_rows // 16, scale_rows, 0)
 
     ids_row = ids_row_ref[...]
     expert_col = lax.broadcasted_iota(jnp.int32, (n_ep, tok_rows), 0)
@@ -184,8 +207,6 @@
 
     pl.semaphore_wait(barrier, n_ep - 1 + 2)
 
-    own_cols = pl.ds(pl.multiple_of(tp * cols, cols), cols)
-
     def z_copy(k, c):
         return pltpu.make_async_remote_copy(
             src_ref=outbox.at[k - 1, c],
@@ -214,6 +235,14 @@
                 preferred_element_type=jnp.float32,
             ).astype(jnp.bfloat16)
             z_copy(k, c).start()
+
+    def norm_rows(i, carry):
+        rows = pl.ds(pl.multiple_of(i * 16, 16), 16)
+        values = tokens_ref[rows, :].astype(jnp.float32)
+        normed[rows, :] = (values * scales[rows, 0:1] * gain_ref[...]).astype(jnp.bfloat16)
+        return carry
+
+    lax.fori_loop(0, tok_rows // 16, norm_rows, 0)
 
     partner = flip(ep, 1)
     pair_copy = pltpu.make_async_remote_copy(
@@ -329,7 +358,6 @@
             return carry
 
         lax.fori_loop(0, hid // COLUMN_TILE, tile, 0)
-        spread(1, k)
 
     def back_copy(k, c):
         return pltpu.make_async_remote_copy(
@@ -381,39 +409,39 @@
     pair_arrival.wait_recv()
     units(0)
     enter(1)
-    relay(1, 0)
+    relay(0, 1)
     if pairs > 2:
         enter(2)
-    relay(0, 1)
     loads[2].wait()
-    gathered(1, 0)
-    results(0)
     for k in range(1, pairs):
         gathered(0, k)
         units(k)
+        spread(1, k)
+        if k + 1 < pairs:
+            relay(0, k + 1)
         if k + 2 < pairs:
             enter(k + 2)
-        if k + 1 < pairs:
-            relay(0, k + 1)
-            relay(1, k)
+        if k == pairs - 1:
+            spread(1, 0)
         if k >= 2:
             gathered(1, k - 1)
             results(k - 1)
-    relay(1, pairs - 1)
+        relay(1, k)
     gathered(1, pairs - 1)
     results(pairs - 1)
-
-    expert_row = lax.broadcasted_iota(jnp.int32, (tok_rows, n_ep), 1)
-    ids = [ids_ref[:, k : k + 1] for k in range(2)]
-    hits = ((ids[0] == expert_row) | (ids[1] == expert_row)).astype(jnp.float32).astype(jnp.bfloat16)
-    later = (second < first).astype(jnp.float32).astype(jnp.bfloat16)
-    before = jnp.dot(later, hits, preferred_element_type=jnp.float32)
-    place = lax.broadcasted_iota(jnp.int32, (tok_rows, n_ep * slots), 1).astype(jnp.float32)
-    chosen = []
+    relay(1, 0)
+    gathered(1, 0)
+    results(0)
+
+    place = lax.broadcasted_iota(jnp.int32, (n_ep * slots, tok_rows), 0).astype(jnp.float32)
+    share = None
     for k in range(2):
-        slot = jnp.sum(jnp.where(ids[k] == expert_row, before, 0.0), axis=1, keepdims=True)
-        spot = ids[k].astype(jnp.float32) * slots + slot
-        chosen.append((place == spot).astype(jnp.float32).astype(jnp.bfloat16))
+        spot = ids_row[k : k + 1, :].astype(jnp.float32) * slots + slot_row[k]
+        part = jnp.where(place == spot, route_row_ref[k : k + 1, :], 0.0)
+        share = part if share is None else share + part
+    share = jnp.transpose(share)
+    share_high = share.astype(jnp.bfloat16)
+    share_low = (share - share_high.astype(jnp.float32)).astype(jnp.bfloat16)
 
     for flips in range(1, n_ep):
         back_arrival(flips).wait_recv()
@@ -421,11 +449,8 @@
     def mix(i, carry):
         where = pl.ds(pl.multiple_of(i * COLUMN_TILE, COLUMN_TILE), COLUMN_TILE)
         table = back[:, :, where].reshape(n_ep * slots, COLUMN_TILE)
-        total = None
-        for k in range(2):
-            part = jnp.dot(chosen[k], table, preferred_element_type=jnp.float32)
-            part = part * route_ref[:, k : k + 1]
-            total = part if total is None else total + part
+        total = jnp.dot(share_high, table, preferred_element_type=jnp.float32)
+        total = total + jnp.dot(share_low, table, preferred_element_type=jnp.float32)
         out_ref[:, where] = total.astype(jnp.bfloat16)
         return carry
 
@@ -457,17 +482,31 @@
     cols = width // n_tp
     pairs = n_ep // 2
     vmem = pl.BlockSpec(memory_space=pltpu.VMEM)
-    hbm = pl.BlockSpec(memory_space=pl.ANY)
+    hbm = pl.BlockSpec(memory_space=pltpu.HBM)
     dma = pltpu.SemaphoreType.DMA
+    arrays = (
+        tokens,
+        jnp.transpose(expert_ids),
+        jnp.transpose(route_weight),
+        norm_gain.reshape(1, width),
+        gate_weight,
+        up_weight,
+        down_weight,
+    )
     return pl.pallas_call(
         functools.partial(fused_kernel, n_ep, n_tp, slots),
         out_shape=jax.ShapeDtypeStruct((tok_rows, outs), jnp.bfloat16),
-        in_specs=[vmem] * 5 + [hbm] * 3,
+        in_specs=[hbm] * 7,
         out_specs=vmem,
         scratch_shapes=[
+            pltpu.VMEM(tokens.shape, tokens.dtype),
+            pltpu.VMEM(expert_ids.shape[::-1], expert_ids.dtype),
+            pltpu.VMEM(route_weight.shape[::-1], route_weight.dtype),
+            pltpu.VMEM((1, width), norm_gain.dtype),
             pltpu.VMEM(gate_weight.shape[1:], jnp.bfloat16),
             pltpu.VMEM(up_weight.shape[1:], jnp.bfloat16),
             pltpu.VMEM(down_weight.shape[1:], jnp.bfloat16),
+            pltpu.VMEM((tok_rows, 128), jnp.float32),
             pltpu.VMEM((tok_rows, width), jnp.bfloat16),
             pltpu.VMEM((pairs - 1, 2, slots, cols), jnp.bfloat16),
             pltpu.VMEM((n_tp, slots, cols), jnp.bfloat16),
@@ -475,6 +514,7 @@
             pltpu.VMEM((pairs, n_tp, 2, slots, hid), jnp.bfloat16),
             pltpu.VMEM((pairs, 2, slots, outs), jnp.bfloat16),
             pltpu.VMEM((n_ep, slots, outs), jnp.bfloat16),
+            dma((4,)),
             dma((3,)),
             dma((pairs, 2)),
             dma((pairs, 2)),
@@ -488,16 +528,7 @@
         compiler_params=pltpu.CompilerParams(
             collective_id=0, has_side_effects=True, vmem_limit_bytes=VMEM_BYTES
         ),
-    )(
-        tokens,
-        expert_ids,
-        jnp.transpose(expert_ids),
-        route_weight,
-        norm_gain.reshape(1, width),
-        gate_weight,
-        up_weight,
-        down_weight,
-    )
+    )(*(pltpu.with_memory_space_constraint(array, pltpu.HBM) for array in arrays))
 
 
 def slots_of(n_ep, token_shape, id_shape):

time: 102 us -> 94.3 us (0.925)
  the two profiles are of different devices: /device:TPU:19 before, /device:TPU:0 now
where the time goes in v2:
time: 94.3 us; the launch traced here: 93.7 us
  Pallas kernels  93 us (99%)
    pallas_call x1, Pallas kernels, fused_path(): pl.pallas_call(functools.partial(fused_kernel, n_ep, n_tp, slots), out_sh...  93 us

profile of v2, /device:TPU:0, one launch (start us, length us, event | category | flops | bytes accessed | tf_op | source)
XLA Modules:
  0.0 93.7 jit_solution(223502599656467812)
XLA Ops:
  0.0 93.0 %shard_map.73 = bf16[192,1024]{1,0:T(8,128)(2,1)S(1)} custom-call(bf16[192,4096]{1,0:T(8,128)(2,1)} %tokens_hbm.1, s32[2,192]{1,0:T(2,128)} %bitcast.4, f32[2,192]{1,0:T(2,128)} %bitcast.5, f32[1,4096]{1,0:T(1,128)} %bitcast.3, bf16[1,4096,1024]{2,1,0:T(8,128)(2,1)} %gate_hbm.1, bf16[1,4096,1024]{2,1,0:T(8,128)(2,1)} %up_hbm.1, bf16[1,4096,1024]{2,1,0:T(8,128)(2,1)} %down_hbm.1), custom_call_target="tpu_custom_call" | custom-call | tf_op jit(solution)/shard_map/pallas_call | solution.py:496
  93.0 0.7 copy.9

commit v3 on v2

--- a/solution.py
+++ b/solution.py
@@ -77,7 +77,7 @@
     return mixed.astype(jnp.bfloat16)
 
 
-VMEM_BYTES = 46 * 1024 * 1024
+VMEM_BYTES = 48 * 1024 * 1024
 COLUMN_TILE = 256
 
 
@@ -174,15 +174,15 @@
     own_cols = pl.ds(pl.multiple_of(tp * cols, cols), cols)
 
     def scale_rows(i, carry):
-        rows = pl.ds(pl.multiple_of(i * 16, 16), 16)
+        rows = pl.ds(pl.multiple_of(i * 32, 32), 32)
         values = tokens_ref[rows, :].astype(jnp.float32)
         scale = lax.rsqrt(jnp.mean(values * values, axis=-1, keepdims=True) + EPS)
-        scales[rows, :] = jnp.broadcast_to(scale, (16, scales.shape[1]))
+        scales[rows, :] = jnp.broadcast_to(scale, (32, scales.shape[1]))
         values = tokens_ref[rows, own_cols].astype(jnp.float32)
         normed[rows, own_cols] = (values * scale * gain_ref[:, own_cols]).astype(jnp.bfloat16)
         return carry
 
-    lax.fori_loop(0, tok_rows // 16, scale_rows, 0)
+    lax.fori_loop(0, tok_rows // 32, scale_rows, 0)
 
     ids_row = ids_row_ref[...]
     expert_col = lax.broadcasted_iota(jnp.int32, (n_ep, tok_rows), 0)
@@ -209,7 +209,7 @@
 
     def z_copy(k, c):
         return pltpu.make_async_remote_copy(
-            src_ref=outbox.at[k - 1, c],
+            src_ref=outbox.at[k - 2, c],
             dst_ref=xbuf.at[k, tp, core],
             send_sem=z_send.at[k, c],
             recv_sem=z_recv.at[k, core],
@@ -219,7 +219,7 @@
 
     def z_arrival(k, c):
         return pltpu.make_async_remote_copy(
-            src_ref=outbox.at[k - 1, c],
+            src_ref=outbox.at[k - 2, c],
             dst_ref=xbuf.at[k, tp, c],
             send_sem=z_send.at[k, c],
             recv_sem=z_recv.at[k, c],
@@ -227,13 +227,15 @@
             device_id_type=pl.DeviceIdType.MESH,
         )
 
-    for k in range(1, pairs):
-        for c in range(2):
-            outbox[k - 1, c] = jnp.dot(
-                pick_of(flip(pair, k) * 2 + c),
-                normed[:, own_cols],
-                preferred_element_type=jnp.float32,
-            ).astype(jnp.bfloat16)
+    away = [(k, c) for k in range(2, pairs) for c in range(2)]
+    if away:
+        picks = jnp.concatenate([pick_of(flip(pair, k) * 2 + c) for k, c in away], axis=0)
+        rows_out = jnp.dot(
+            picks, normed[:, own_cols], preferred_element_type=jnp.float32
+        ).astype(jnp.bfloat16)
+        for at, (k, c) in enumerate(away):
+            outbox[k - 2, c] = rows_out[at * slots : (at + 1) * slots]
+        for k, c in away:
             z_copy(k, c).start()
 
     def norm_rows(i, carry):
@@ -246,7 +248,7 @@
 
     partner = flip(ep, 1)
     pair_copy = pltpu.make_async_remote_copy(
-        src_ref=fullbox,
+        src_ref=fullbox.at[2],
         dst_ref=xbuf.at[0, :, core],
         send_sem=pair_send,
         recv_sem=pair_recv,
@@ -254,98 +256,129 @@
         device_id_type=pl.DeviceIdType.MESH,
     )
     pair_arrival = pltpu.make_async_remote_copy(
-        src_ref=fullbox,
+        src_ref=fullbox.at[2],
         dst_ref=xbuf.at[0, :, 1 - core],
         send_sem=pair_send,
         recv_sem=pair_recv,
         device_id=(partner, tp),
         device_id_type=pl.DeviceIdType.MESH,
     )
-    theirs = pick_of(partner)
+
+    def whole_copy(c):
+        return pltpu.make_async_remote_copy(
+            src_ref=fullbox.at[c],
+            dst_ref=xbuf.at[1, :, core],
+            send_sem=z_send.at[1, c],
+            recv_sem=z_recv.at[1, core],
+            device_id=(flip(pair, 1) * 2 + c, tp),
+            device_id_type=pl.DeviceIdType.MESH,
+        )
+
+    def whole_arrival(c):
+        return pltpu.make_async_remote_copy(
+            src_ref=fullbox.at[c],
+            dst_ref=xbuf.at[1, :, c],
+            send_sem=z_send.at[1, c],
+            recv_sem=z_recv.at[1, c],
+            device_id=(flip(pair, 1) * 2 + c, tp),
+            device_id_type=pl.DeviceIdType.MESH,
+        )
+
+    near = flip(pair, 1) * 2
+    picks = jnp.concatenate(
+        [pick_of(near), pick_of(near + 1), pick_of(partner), pick_of(ep)], axis=0
+    )
     for j in range(n_tp):
-        fullbox[j] = jnp.dot(
-            theirs, normed[:, j * cols : (j + 1) * cols], preferred_element_type=jnp.float32
+        whole = jnp.dot(
+            picks, normed[:, j * cols : (j + 1) * cols], preferred_element_type=jnp.float32
         ).astype(jnp.bfloat16)
+        for at in range(3):
+            fullbox[at, j] = whole[at * slots : (at + 1) * slots]
+        xbuf[0, j, core] = whole[3 * slots :]
     pair_copy.start()
-    mine = pick_of(ep)
-    for j in range(n_tp):
-        xbuf[0, j, core] = jnp.dot(
-            mine, normed[:, j * cols : (j + 1) * cols], preferred_element_type=jnp.float32
-        ).astype(jnp.bfloat16)
+    for c in range(2):
+        whole_copy(c).start()
 
     boxes = (xbuf, hbuf)
-
-    def block_copy(b, k, d, half):
-        return pltpu.make_async_remote_copy(
-            src_ref=boxes[b].at[k, tp, half],
-            dst_ref=boxes[b].at[k, tp, half],
-            send_sem=g_send.at[b, k, 2 * d + half],
-            recv_sem=g_recv.at[b, k, 2 * d + half],
+    part_a, part_b = (1 - core, 0), (core, pairs)
+    piece = slots // 2
+
+    def place_of(b, k, j, half, part):
+        if part is None:
+            return boxes[b].at[k, j, half]
+        return boxes[b].at[k, j, part[0], pl.ds(half * piece, piece)]
+
+    def sems_of(b, k, at, part):
+        row = k if part is None else part[1]
+        return {"send_sem": g_send.at[b, row, at], "recv_sem": g_recv.at[b, row, at]}
+
+    def block_copy(b, k, d, half, part):
+        return pltpu.make_async_remote_copy(
+            src_ref=place_of(b, k, tp, half, part),
+            dst_ref=place_of(b, k, tp, half, part),
             device_id=(ep, side[d]),
             device_id_type=pl.DeviceIdType.MESH,
-        )
-
-    def block_arrival(b, k, d, half):
-        return pltpu.make_async_remote_copy(
-            src_ref=boxes[b].at[k, side[d], half],
-            dst_ref=boxes[b].at[k, side[d], half],
-            send_sem=g_send.at[b, k, 2 * d + half],
-            recv_sem=g_recv.at[b, k, 2 * d + half],
+            **sems_of(b, k, 2 * d + half, part),
+        )
+
+    def block_arrival(b, k, d, half, part):
+        return pltpu.make_async_remote_copy(
+            src_ref=place_of(b, k, side[d], half, part),
+            dst_ref=place_of(b, k, side[d], half, part),
             device_id=(ep, side[d]),
             device_id_type=pl.DeviceIdType.MESH,
-        )
-
-    def relay_copy(b, k, d):
-        return pltpu.make_async_remote_copy(
-            src_ref=boxes[b].at[k, side[d], d],
-            dst_ref=boxes[b].at[k, side[d], d],
-            send_sem=g_send.at[b, k, 4 + d],
-            recv_sem=g_recv.at[b, k, 4 + d],
+            **sems_of(b, k, 2 * d + half, part),
+        )
+
+    def relay_copy(b, k, d, part):
+        return pltpu.make_async_remote_copy(
+            src_ref=place_of(b, k, side[d], d, part),
+            dst_ref=place_of(b, k, side[d], d, part),
             device_id=(ep, side[1 - d]),
             device_id_type=pl.DeviceIdType.MESH,
-        )
-
-    def relay_arrival(b, k, d):
-        return pltpu.make_async_remote_copy(
-            src_ref=boxes[b].at[k, far, d],
-            dst_ref=boxes[b].at[k, far, d],
-            send_sem=g_send.at[b, k, 4 + d],
-            recv_sem=g_recv.at[b, k, 4 + d],
+            **sems_of(b, k, 4 + d, part),
+        )
+
+    def relay_arrival(b, k, d, part):
+        return pltpu.make_async_remote_copy(
+            src_ref=place_of(b, k, far, d, part),
+            dst_ref=place_of(b, k, far, d, part),
             device_id=(ep, side[1 - d]),
             device_id_type=pl.DeviceIdType.MESH,
-        )
-
-    def spread(b, k):
+            **sems_of(b, k, 4 + d, part),
+        )
+
+    def spread(b, k, part=None):
         for step in range(2):
             for d in range(2):
-                block_copy(b, k, d, d if step == 0 else 1 - d).start()
-
-    def relay(b, k):
+                block_copy(b, k, d, d if step == 0 else 1 - d, part).start()
+
+    def relay(b, k, part=None):
         for d in range(2):
-            block_arrival(b, k, d, d).wait_recv()
-            relay_copy(b, k, d).start()
-
-    def gathered(b, k):
+            block_arrival(b, k, d, d, part).wait_recv()
+            relay_copy(b, k, d, part).start()
+
+    def gathered(b, k, part=None):
         for d in range(2):
-            block_arrival(b, k, d, 1 - d).wait_recv()
+            block_arrival(b, k, d, 1 - d, part).wait_recv()
         for d in range(2):
-            relay_arrival(b, k, d).wait_recv()
+            relay_arrival(b, k, d, part).wait_recv()
 
     def enter(k):
         for c in range(2):
             z_arrival(k, c).wait_recv()
         spread(0, k)
 
-    def dot_blocks(box, k, weight, where):
+    def dot_blocks(box, k, weight, where, part=None):
         depth = box.shape[-1]
         total = None
         for j in range(n_tp):
-            part = jnp.dot(
-                box[k, j].reshape(2 * slots, depth),
+            term = jnp.dot(
+                box[k, j].reshape(2 * slots, depth) if part is None else box[k, j, part[0]],
                 weight[j * depth : (j + 1) * depth, where],
                 preferred_element_type=jnp.float32,
             )
-            total = part if total is None else total + part
+            total = term if total is None else total + term
         return total
 
     def units(k):
@@ -381,7 +414,7 @@
         )
 
     partner_back = pltpu.make_async_remote_copy(
-        src_ref=obuf.at[0, 1 - core],
+        src_ref=obuf.at[0, 0],
         dst_ref=back.at[ep],
         send_sem=b_send.at[0, 0],
         recv_sem=b_recv.at[ep],
@@ -397,41 +430,64 @@
             return carry
 
         lax.fori_loop(0, outs // COLUMN_TILE, tile, 0)
-        if k == 0:
-            partner_back.start()
-            back[ep] = obuf[0, core]
-        else:
-            for c in range(2):
-                back_copy(k, c).start()
+        for c in range(2):
+            back_copy(k, c).start()
+
+    def own_results(part, store):
+        def tile(i, carry):
+            where = pl.ds(pl.multiple_of(i * COLUMN_TILE, COLUMN_TILE), COLUMN_TILE)
+            store(where, dot_blocks(hbuf, 0, down_v, where, part).astype(jnp.bfloat16))
+            return carry
+
+        lax.fori_loop(0, outs // COLUMN_TILE, tile, 0)
+
+    def store_partner(where, total):
+        obuf[0, 0, :, where] = total
+
+    def store_own(where, total):
+        back[ep, :, where] = total
 
     loads[0].wait()
     loads[1].wait()
     pair_arrival.wait_recv()
     units(0)
-    enter(1)
-    relay(0, 1)
+    spread(1, 0, part_a)
     if pairs > 2:
         enter(2)
+    relay(1, 0, part_a)
     loads[2].wait()
-    for k in range(1, pairs):
+    gathered(1, 0, part_a)
+    own_results(part_a, store_partner)
+    partner_back.start()
+    for k in range(2, pairs):
+        if k == 2:
+            relay(0, k)
+        if k + 1 < pairs:
+            enter(k + 1)
         gathered(0, k)
         units(k)
-        spread(1, k)
         if k + 1 < pairs:
             relay(0, k + 1)
-        if k + 2 < pairs:
-            enter(k + 2)
-        if k == pairs - 1:
-            spread(1, 0)
-        if k >= 2:
+        spread(1, k)
+        if k > 2:
+            relay(1, k - 1)
             gathered(1, k - 1)
             results(k - 1)
-        relay(1, k)
-    gathered(1, pairs - 1)
-    results(pairs - 1)
-    relay(1, 0)
-    gathered(1, 0)
-    results(0)
+    for c in range(2):
+        whole_arrival(c).wait_recv()
+    units(1)
+    spread(1, 1)
+    spread(1, 0, part_b)
+    if pairs > 2:
+        relay(1, pairs - 1)
+        gathered(1, pairs - 1)
+        results(pairs - 1)
+    relay(1, 1)
+    gathered(1, 1)
+    results(1)
+    relay(1, 0, part_b)
+    gathered(1, 0, part_b)
+    own_results(part_b, store_own)
 
     place = lax.broadcasted_iota(jnp.int32, (n_ep * slots, tok_rows), 0).astype(jnp.float32)
     share = None
@@ -458,18 +514,19 @@
 
     for k in range(1, pairs):
         for c in range(2):
-            z_copy(k, c).wait_send()
+            if k > 1:
+                z_copy(k, c).wait_send()
+            else:
+                whole_copy(c).wait_send()
             back_copy(k, c).wait_send()
     pair_copy.wait_send()
     partner_back.wait_send()
-    for k in range(pairs):
-        for b in range(2):
-            if b == 0 and k == 0:
-                continue
-            for d in range(2):
-                for half in range(2):
-                    block_copy(b, k, d, half).wait_send()
-                relay_copy(b, k, d).wait_send()
+    sent = [(0, k, None) for k in range(2, pairs)] + [(1, k, None) for k in range(1, pairs)]
+    for b, k, part in sent + [(1, 0, part_a), (1, 0, part_b)]:
+        for d in range(2):
+            for half in range(2):
+                block_copy(b, k, d, half, part).wait_send()
+            relay_copy(b, k, d, part).wait_send()
 
 
 def fused_path(
@@ -508,8 +565,8 @@
             pltpu.VMEM(down_weight.shape[1:], jnp.bfloat16),
             pltpu.VMEM((tok_rows, 128), jnp.float32),
             pltpu.VMEM((tok_rows, width), jnp.bfloat16),
-            pltpu.VMEM((pairs - 1, 2, slots, cols), jnp.bfloat16),
-            pltpu.VMEM((n_tp, slots, cols), jnp.bfloat16),
+            pltpu.VMEM((max(pairs - 2, 1), 2, slots, cols), jnp.bfloat16),
+            pltpu.VMEM((3, n_tp, slots, cols), jnp.bfloat16),
             pltpu.VMEM((pairs, n_tp, 2, slots, cols), jnp.bfloat16),
             pltpu.VMEM((pairs, n_tp, 2, slots, hid), jnp.bfloat16),
             pltpu.VMEM((pairs, 2, slots, outs), jnp.bfloat16),
@@ -520,8 +577,8 @@
             dma((pairs, 2)),
             dma,
             dma,
-            dma((2, pairs, 6)),
-            dma((2, pairs, 6)),
+            dma((2, pairs + 1, 6)),
+            dma((2, pairs + 1, 6)),
             dma((pairs, 2)),
             dma((n_ep,)),
         ],
@@ -533,14 +590,14 @@
 
 def slots_of(n_ep, token_shape, id_shape):
     capacity = 5 * token_shape[0] * id_shape[1] // (4 * n_ep)
-    return -(-capacity // 16) * 16
+    return -(-capacity // 32) * 32
 
 
 def on_device(tokens, expert_ids, route_weight, norm_gain, gate_weight, up_weight, down_weight):
     n_ep = lax.axis_size("ep")
     n_tp = lax.axis_size("tp")
     args = (tokens, expert_ids, route_weight, norm_gain, gate_weight, up_weight, down_weight)
-    fits = n_tp == 4 and n_ep >= 4 and n_ep & (n_ep - 1) == 0 and gate_weight.shape[0] == 1
+    fits = n_tp == 4 and tokens.shape[0] % 32 == 0 and n_ep >= 4 and n_ep & (n_ep - 1) == 0 and gate_weight.shape[0] == 1
     if fits and expert_ids.shape[1] == 2:
         return fused_path(n_ep, n_tp, *args)
     return plain_path(*args)

time: 94.3 us -> 101 us (1.071)
  Pallas kernels: 93 us -> 99.7 us
    pallas_call x1, Pallas kernels: 93 us -> 99.7 us  [fused_path(): pl.pallas_call(functools.partial(fused_kernel, n_ep, n_tp, slots), out_sh...]
where the time goes in v3:
time: 101 us; the launch traced here: 100 us
  Pallas kernels  99.7 us (99%)
    pallas_call x1, Pallas kernels, fused_path(): pl.pallas_call(functools.partial(fused_kernel, n_ep, n_tp, slots), out_sh...  99.7 us

profile of v3, /device:TPU:0, one launch (start us, length us, event | category | flops | bytes accessed | tf_op | source)
XLA Modules:
  0.0 100.5 jit_solution(5529278202136889297)
XLA Ops:
  0.0 99.7 %shard_map.73 = bf16[192,1024]{1,0:T(8,128)(2,1)S(1)} custom-call(bf16[192,4096]{1,0:T(8,128)(2,1)} %tokens_hbm.1, s32[2,192]{1,0:T(2,128)} %bitcast.4, f32[2,192]{1,0:T(2,128)} %bitcast.5, f32[1,4096]{1,0:T(1,128)} %bitcast.3, bf16[1,4096,1024]{2,1,0:T(8,128)(2,1)} %gate_hbm.1, bf16[1,4096,1024]{2,1,0:T(8,128)(2,1)} %up_hbm.1, bf16[1,4096,1024]{2,1,0:T(8,128)(2,1)} %down_hbm.1), custom_call_target="tpu_custom_call" | custom-call | tf_op jit(solution)/shard_map/pallas_call | solution.py:553
  99.8 0.7 copy.9
